TPU v7x, 512 devices: a whole 4x4x16 slice. The times are simulated.
512 devices in a mesh: ep: 32 (over z, core), tp: 16 (over y, x).
Axes of the slice: x: 4, y: 4, z: 16, core: 2. Of those that a mesh axis runs over, the one named last changes fastest.
Arguments:
- conv_input: bfloat16 [1024, 65536], P('tp', 'ep'), may hold values from -6 to 6
- out_gate: bfloat16 [1024, 65536], P('tp', 'ep'), may hold values from -6 to 6
- in_gate: bfloat16 [1024, 65536], P('tp', 'ep'), may hold values from -6 to 6
- conv_taps: float32 [3, 1024], replicated, may hold values from -3.5 to 3.5
- mixer_proj: bfloat16 [1024, 2048], P(None, 'tp'), may hold values from -0.1875 to 0.1875
- token_rows: bfloat16 [8192, 2048], P('ep', 'tp'), may hold values from -4000 to 4000
- routes: int32 [8192, 2], P('ep'), may hold values from 0 to 31, as said below
- route_weights: float32 [8192, 2], P('ep'), may hold values from 0.3 to 1
- expert_gate: bfloat16 [32, 2048, 4096], P('ep', None, 'tp'), may hold values from -0.125 to 0.125
- expert_up: bfloat16 [32, 2048, 4096], P('ep', None, 'tp'), may hold values from -0.125 to 0.125
- expert_down: bfloat16 [32, 4096, 2048], P('ep', 'tp'), may hold values from -0.125 to 0.125
Outputs:
- mixed_out: bfloat16 [65536, 2048], P('ep', 'tp')
- expert_out: bfloat16 [8192, 2048], P('ep', 'tp')
Inputs may be any that keep to these rules, and one draw needn't show every extreme that they name: `routes`: in each aligned block of 256 rows, no expert is named more than 32 times and one expert, the same in every block, exactly 32 times; the two experts of a row differ.
All inputs are finite; a program needn't handle non-finite values.
Results may differ from a plain program's by a relative error of at most 0.015.
Values may be sent and summed in bfloat16 or wider, within the bound.
A program may use at most 64 MiB of HBM per device.

v0:
```python
import jax
import jax.numpy as jnp
from jax import lax
from jax.sharding import PartitionSpec as P

KERNEL = 3


EPSILON = 1e-06


def passed_along(value, axis, by):
    devices = lax.axis_size(axis)
    pairs = [(i, i + by) for i in range(devices) if 0 <= i + by < devices]
    return lax.ppermute(value, axis, pairs)


def split_up(value, dim, devices):
    before, after = (value.shape[:dim], value.shape[dim + 1 :])
    return jnp.moveaxis(value.reshape(*before, devices, -1, *after), dim, 0)


def sent_and_summed(value, axis, dim):
    blocks = split_up(value, dim, lax.axis_size(axis))
    arrived = lax.all_to_all(blocks, axis, split_axis=0, concat_axis=0, tiled=True)
    return arrived.astype(jnp.float32).sum(axis=0)


def slot_places(route_ids, capacity, experts):
    flat_ids = route_ids.reshape(-1)
    hit_table = (flat_ids[:, None] == jnp.arange(experts, dtype=jnp.int32)[None, :]).astype(
        jnp.int32
    )
    earlier = jnp.cumsum(hit_table, axis=0) - hit_table
    slot_rank = jnp.sum(earlier * hit_table, axis=1)
    return flat_ids * capacity + slot_rank


def body(
    conv_input,
    out_gate,
    in_gate,
    conv_taps,
    mixer_proj,
    token_rows,
    routes,
    route_weights,
    expert_gate,
    expert_up,
    expert_down,
):
    width_part = conv_input.shape[0]
    length = conv_input.shape[1]
    offset = lax.axis_index("tp") * width_part
    local_taps = lax.dynamic_slice_in_dim(conv_taps, offset, width_part, 1)
    z_rows = (conv_input.astype(jnp.float32) * in_gate.astype(jnp.float32)).astype(jnp.bfloat16)
    rim_rows = passed_along(z_rows[:, length - (KERNEL - 1) :], "ep", 1)
    longer = jnp.concatenate([rim_rows, z_rows], axis=1).astype(jnp.float32)
    conv_sum = jnp.zeros(z_rows.shape, jnp.float32)
    for lag_index in range(KERNEL):
        begin = KERNEL - 1 - lag_index
        conv_sum = conv_sum + local_taps[lag_index][:, None] * longer[:, begin : begin + length]
    gated = (out_gate.astype(jnp.float32) * conv_sum).astype(jnp.bfloat16)
    mixed_sum = lax.dot_general(
        lax.all_gather(gated, "tp", axis=0, tiled=True),
        mixer_proj,
        (((0,), (0,)), ((), ())),
        preferred_element_type=jnp.float32,
    )
    mixed_out = mixed_sum.astype(jnp.bfloat16)
    experts = lax.axis_size("ep")
    rows_b = token_rows.shape[0]
    cols_part = token_rows.shape[1]
    capacity = 4 * rows_b // experts
    slot_total = experts * capacity
    places = slot_places(routes, capacity, experts)
    sources = jnp.arange(2 * rows_b, dtype=jnp.int32) // 2
    gate_weight = expert_gate[0]
    up_weight = expert_up[0]
    down_weight = expert_down[0]
    feature_count = cols_part * lax.axis_size("tp")
    buffer = jnp.zeros((slot_total, cols_part), jnp.bfloat16).at[places].set(token_rows[sources])
    arrived = lax.all_to_all(
        buffer.reshape(experts, capacity, cols_part), "ep", split_axis=0, concat_axis=0, tiled=True
    )
    arrived = arrived.reshape(slot_total, cols_part)
    part_in = lax.all_gather(arrived, "tp", axis=1, tiled=True)
    gate_sum = jnp.dot(part_in, gate_weight, preferred_element_type=jnp.float32)
    up_sum = jnp.dot(part_in, up_weight, preferred_element_type=jnp.float32)
    squares = jnp.sum(jnp.square(part_in.astype(jnp.float32)), axis=1)
    row_scale = lax.rsqrt(squares / feature_count + EPSILON)[:, None]
    hidden = (jax.nn.silu(row_scale * gate_sum) * (row_scale * up_sum)).astype(jnp.bfloat16)
    summed = sent_and_summed(
        lax.dot_general(
            down_weight, hidden, (((0,), (1,)), ((), ())), preferred_element_type=jnp.float32
        ).astype(jnp.bfloat16),
        "tp",
        0,
    )
    expert_rows = summed.astype(jnp.bfloat16).reshape(cols_part, experts, capacity)
    returned = lax.all_to_all(expert_rows, "ep", split_axis=1, concat_axis=1, tiled=True).reshape(
        cols_part, slot_total
    )
    picked = returned[:, places].astype(jnp.float32).reshape(cols_part, rows_b, 2)
    combined = jnp.sum(picked * route_weights[None, :, :], axis=2)
    expert_out = combined.T.astype(jnp.bfloat16)
    return (mixed_out, expert_out)


def solution(mesh):
    return jax.shard_map(
        body,
        mesh=mesh,
        in_specs=(
            P("tp", "ep"),
            P("tp", "ep"),
            P("tp", "ep"),
            P(),
            P(None, "tp"),
            P("ep", "tp"),
            P("ep", None),
            P("ep", None),
            P("ep", None, "tp"),
            P("ep", None, "tp"),
            P("ep", "tp", None),
        ),
        out_specs=(P("ep", "tp"), P("ep", "tp")),
        check_vma=False,
    )
```

profile of v0, /device:TPU:1, one launch (start us, length us, event | category | flops | bytes accessed | tf_op | source)
XLA Modules:
  0.0 242.8 jit_solution(143505425020026601)
XLA Ops:
  7.2 0.0 copy-start
  7.2 0.0 all-gather.5.cloned.1.call-start
  7.2 0.9 copy.26
  8.1 0.1 eq.29
  8.3 0.1 eq.25
  8.4 0.7 broadcast_multiply_fusion
  9.1 1.2 reduce-window.6
  10.3 0.2 slice_reduce_fusion
  10.6 0.1 copy.25
  10.7 0.1 mul.101
  10.9 0.1 fusion.18
  11.0 4.9 %scatter_custom_fusion = bf16[1024,128]{1,0:T(8,128)(2,1)S(1)} fusion(s32[512]{0:T(512)S(1)} %bitcast.65, bf16[256,128]{1,0:T(8,128)(2,1)} %param.16, s32[1024]{0:T(1024)S(1)} %pad_clamp_fusion.1, bf16[]{:T(256)} %constant.39.clone.1), kind=kCustom, calls=%fused_computation.26 | custom fusion | bytes 262656 | tf_op jit(solution)/shard_map/scatter | solution.py:82
  15.9 38.9 %all_to_all.15 = bf16[32,32,128]{2,1,0:T(8,128)(2,1)} all-to-all(bf16[32,32,128]{2,1,0:T(8,128)(2,1)S(1)} %bitcast.63), channel_id=1, replica_groups=mesh['ep'=32,'tp'=16] {'ep'}, dimensions={0} | all-to-all | bytes 524288 | tf_op jit(solution)/shard_map/all_to_all | solution.py:83
  54.8 0.0 copy-start.3
  54.8 0.0 all-gather.5.cloned.1.call-update
  54.8 0.0 all-gather.3.cloned.1.call-start
  54.9 1.2 multiply_convert_fusion
  56.0 0.1 slice.40
  56.1 2.2 collective-permute-start
  58.4 0.8 constant_dynamic-slice_fusion
  59.1 0.1 collective-permute-done
  59.2 0.1 maximum_convert_fusion
  59.4 2.0 fusion.9
  61.4 0.0 all-gather.3.cloned.1.call-update
  61.4 55.6 %all-gather.5.cloned.1.call-done = bf16[1024,2048]{1,0:T(8,128)(2,1)} async-done(((bf16[1024,128]{1,0:T(8,128)(2,1)}), bf16[1024,2048]{1,0:T(8,128)(2,1)}) %all-gather.5.cloned.1.call-update) | async-done | bytes 4194320 | tf_op jit(solution)/shard_map/all_gather | solution.py:87
  117.1 0.0 copy-start.1
  117.1 3.2 %multiply_reduce_fusion = f32[1024]{0:T(1024)S(1)} fusion(bf16[1024,2048]{1,0:T(8,128)(2,1)} %all-gather.5.cloned.1.call-done), kind=kLoop, calls=%fused_computation.3 | loop fusion | flops 6290432 | bytes 4198400 | tf_op jit(solution)/shard_map/reduce_sum | solution.py:90
  120.3 0.0 copy-start.4
  120.3 0.0 copy-done.3
  120.3 0.2 copy-done.1
  120.5 2.3 convolution_multiply_fusion.1
  122.8 0.0 copy-done
  122.8 0.0 copy-done.4
  122.8 8.8 %convert_bitcast_fusion = bf16[128,16,8,128]{3,2,1,0:T(8,128)(2,1)} fusion(bf16[1,256,2048]{2,1,0:T(8,128)(2,1)S(1)} %copy-done, bf16[1024,2048]{1,0:T(8,128)(2,1)} %all-gather.5.cloned.1.call-done, bf16[1,2048,256]{2,1,0:T(8,128)(2,1)S(1)} %copy-done.4, f32[1024,256]{1,0:T(8,128)} %convolution_multiply_fusion.1, f32[1024]{0:T(1024)S(1)} %add_rsqrt_fusion), kind=kOutput, calls=%fused_computation.5 | convolution fusion | flops 2151415808 | bytes 11538432 | tf_op jit(solution)/shard_map/dot_general | solution.py:94
  131.6 3.3 %copy.35 = bf16[128,16,8,128]{3,2,0,1:T(8,128)(2,1)S(1)} copy(bf16[128,16,8,128]{3,2,1,0:T(8,128)(2,1)} %convert_bitcast_fusion) | data formatting | bytes 8388608 | tf_op jit(solution)/shard_map/reshape | solution.py:20
  134.9 58.8 %all_to_all.16 = bf16[16,128,1024]{1,2,0:T(8,128)(2,1)} all-to-all(bf16[16,128,1024]{1,2,0:T(8,128)(2,1)S(1)} %bitcast.59), channel_id=1, replica_groups=mesh['ep'=32,'tp'=16] {'tp'}, dimensions={0} | all-to-all | bytes 8388608 | tf_op jit(solution)/shard_map/all_to_all | solution.py:25
  193.7 0.0 copy-start.2
  193.7 0.0 copy-start.5
  193.7 3.9 %reduce_sum.44 = bf16[128,1024]{0,1:T(8,128)(2,1)} reduce(bf16[16,128,1024]{1,2,0:T(8,128)(2,1)} %all_to_all.16, bf16[]{:T(256)} %constant.39.clone.1), dimensions={0}, to_apply=%region_5.6 | reduce | flops 1966080 | bytes 4456450 | tf_op jit(solution)/shard_map/reduce_sum | solution.py:26
  197.6 13.7 %all-to-all-start.2 = ((bf16[128,32,32]{0,2,1:T(8,128)(2,1)}), bf16[128,32,32]{0,2,1:T(8,128)(2,1)S(1)}, u32[]{:S(2)}, u32[]{:S(2)}) async-start(bf16[128,32,32]{0,2,1:T(8,128)(2,1)} %bitcast.13), calls=%async_computation.2 | async-start | bytes 524288 | tf_op jit(solution)/shard_map/all_to_all | solution.py:101
  211.3 0.0 copy-done.2
  211.3 0.1 copy.30
  211.5 3.2 %all-gather.3.cloned.1.call-done = bf16[1024,2048]{1,0:T(8,128)(2,1)} async-done(((bf16[64,2048]{1,0:T(8,128)(2,1)}), bf16[1024,2048]{1,0:T(8,128)(2,1)}) %all-gather.3.cloned.1.call-update) | async-done | bytes 4194320 | tf_op jit(solution)/shard_map/all_gather | solution.py:65
  214.7 0.0 copy-done.5
  214.7 4.3 %convolution_convert_fusion = bf16[2048,128]{1,0:T(8,128)(2,1)} fusion(bf16[1024,2048]{1,0:T(8,128)(2,1)} %all-gather.3.cloned.1.call-done, bf16[1024,128]{1,0:T(8,128)(2,1)S(1)} %copy-done.5), kind=kOutput, calls=%fused_computation.6 | convolution fusion | flops 537133056 | bytes 4980736 | tf_op jit(solution)/shard_map/dot_general | solution.py:64
  219.0 14.6 %all-to-all-done.2 = bf16[128,32,32]{0,2,1:T(8,128)(2,1)S(1)} async-done(((bf16[128,32,32]{0,2,1:T(8,128)(2,1)}), bf16[128,32,32]{0,2,1:T(8,128)(2,1)S(1)}, u32[]{:S(2)}, u32[]{:S(2)}) %all-to-all-start.2) | async-done | bytes 262176 | tf_op jit(solution)/shard_map/all_to_all | solution.py:101
  233.6 1.3 gather_fusion
  234.9 1.0 multiply_reduce_fusion.1
  (10 shorter events, 0.1 us)
Async XLA Ops:
  7.2 115.7 %copy-start = (bf16[1,256,2048]{2,1,0:T(8,128)(2,1)S(1)}, bf16[1,256,2048]{2,1,0:T(8,128)(2,1)}, u32[]{:S(2)}) copy-start(bf16[1,256,2048]{2,1,0:T(8,128)(2,1)} %param.21) | copy-start | bytes 3145732
  7.2 109.9 %all-gather.5.cloned.1.call-start = ((), (), s32[]{:S(2)}) async-start(), calls=%async_computation.4 | async-start | bytes 4456448 | tf_op jit(solution)/shard_map/all_gather | solution.py:87
  54.8 65.5 %copy-start.3 = (bf16[1,2048,256]{2,1,0:T(8,128)(2,1)S(1)}, bf16[1,2048,256]{2,1,0:T(8,128)(2,1)}, u32[]{:S(2)}) copy-start(bf16[1,2048,256]{2,1,0:T(8,128)(2,1)} %param.19) | copy-start | bytes 3145732
  54.8 159.8 %all-gather.3.cloned.1.call-start = ((), (), s32[]{:S(2)}) async-start(), calls=%async_computation.3 | async-start | bytes 4456448 | tf_op jit(solution)/shard_map/all_gather | solution.py:65
  56.1 3.1 %collective-permute-start = (bf16[64,2]{1,0:T(8,128)(2,1)S(1)}, bf16[64,2]{1,0:T(8,128)(2,1)S(1)}, u32[]{:S(2)}, u32[]{:S(2)}) collective-permute-start(bf16[64,2]{1,0:T(8,128)(2,1)S(1)} %slice.40), channel_id=1, source_target_pairs={{0,16},{16,32},{32,48},{48,64},{64,80},{80,96},{96,112},{112,128},... | collective-permute-start | bytes 776 | tf_op jit(solution)/shard_map/ppermute | solution.py:15
  117.1 3.4 %copy-start.1 = (bf16[1024,2048]{1,0:T(8,128)(2,1)S(1)}, bf16[1024,2048]{1,0:T(8,128)(2,1)}, u32[]{:S(2)}) copy-start(bf16[1024,2048]{1,0:T(8,128)(2,1)} %all-gather.5.cloned.1.call-done) | copy-start | bytes 12582916
  120.3 2.5 %copy-start.4 = (bf16[1,2048,256]{2,1,0:T(8,128)(2,1)S(1)}, bf16[1,2048,256]{2,1,0:T(8,128)(2,1)}, u32[]{:S(2)}) copy-start(bf16[1,2048,256]{2,1,0:T(8,128)(2,1)} %param.20) | copy-start | bytes 3145732
  193.7 17.6 %copy-start.2 = (f32[256,2]{0,1:T(2,128)S(1)}, f32[256,2]{0,1:T(2,128)}, u32[]{:S(2)}) copy-start(f32[256,2]{0,1:T(2,128)} %param.18) | copy-start | bytes 6148
  193.7 21.0 %copy-start.5 = (bf16[1024,128]{1,0:T(8,128)(2,1)S(1)}, bf16[1024,128]{1,0:T(8,128)(2,1)}, u32[]{:S(2)}) copy-start(bf16[1024,128]{1,0:T(8,128)(2,1)} %param.15) | copy-start | bytes 786436
  197.6 35.9 %all-to-all-start.2 = ((bf16[128,32,32]{0,2,1:T(8,128)(2,1)}), bf16[128,32,32]{0,2,1:T(8,128)(2,1)S(1)}, u32[]{:S(2)}, u32[]{:S(2)}) async-start(bf16[128,32,32]{0,2,1:T(8,128)(2,1)} %bitcast.13), calls=%async_computation.2 | async-start | bytes 524288 | tf_op jit(solution)/shard_map/all_to_all | solution.py:101
Sparse Core Ops, SparseCore 0:
  54.9 62.0 all-gather.4
  120.6 93.9 all-gather.2
where the time goes:
time: 243 us
  blocking collectives  97.7 us (40%)
  waiting for transfers between devices  73.6 us (30%)
  starting transfers between devices  16 us (7%)
  matrix products  15.4 us (6%)
  between operations  14.2 us (6%)
  other arithmetic  13.6 us (6%)
  local copies, waits for them, and re-layouts  12.4 us (5%)
    all_to_all x1, blocking collectives, sent_and_summed(): lax.all_to_all(blocks, axis, split_axis=0, concat_axis=0, tiled=True)  58.8 us
    all_gather x1, waiting for transfers between devices, body(): part_in = lax.all_gather(arrived, 'tp', axis=1, tiled=True)  55.6 us
    all_to_all x1, blocking collectives, body(): lax.all_to_all(buffer.reshape(experts, capacity, cols_part), 'ep', split_...  38.9 us
    all_to_all x1, waiting for transfers between devices, body(): lax.all_to_all(expert_rows, 'ep', split_axis=1, concat_axis=1, tiled=True)  14.6 us
    all_to_all x1, starting transfers between devices, body(): lax.all_to_all(expert_rows, 'ep', split_axis=1, concat_axis=1, tiled=True)  13.7 us
    dot_general x1, matrix products, body(): lax.dot_general(down_weight, hidden, (((0,), (1,)), ((), ())), preferred_...  8.82 us
    scatter x1, local copies, waits for them, and re-layouts, body(): jnp.zeros((slot_total, cols_part), jnp.bfloat16).at[places]  4.9 us
  transfers between devices with their start and end apart: 4, of which 4 were waited for; matrix products, arithmetic and copies ran while one was open for 12% of the time, Pallas kernels for 0%

commit v1 on v0

v1 whole, which is shorter than its diff:
```python
import jax
import jax.numpy as jnp
from jax import lax
from jax.experimental import pallas as pl
from jax.experimental.pallas import tpu as pltpu
from jax.sharding import PartitionSpec as P

MESH = pl.DeviceIdType.MESH
EPSILON = 1e-06
F32 = jnp.float32
BF16 = jnp.bfloat16

NZ = 16
NCH = 4
OFFS = [0, 1, 15, 2, 14, 3, 13, 4, 12, 5, 11, 6, 10, 7, 9, 8]
ORDER = {o: n for n, o in enumerate(OFFS)}

PLAN = [
    "M1", "P", "M1", "G0", "P", "M0", "G0", "G1", "M1", "G0", "M0", "G2", "G3", "G1", "G0", "G2",
    "G3", "G1", "G3", "G1", "G2", "G0", "G1", "G3", "S1", "S0", "G2", "G3", "S3", "S1", "G2", "S2",
    "S3", "S1", "S2", "S1", "S3", "S0", "P", "S2", "S3", "S1", "M0", "S0", "S2", "M1", "S3", "M0",
    "S0", "P", "S2", "M1", "M0", "S0", "M1", "M0", "M0", "M1",
]
M_GROUP = [0, 1, 1, 2, 3, 4, 5, 5]


def body(conv_in, out_gate, in_gate, taps, proj, tokens, routes, weights, wg, wu, wd,
         mixed_ref, out_ref,
         ci_v, og_v, ig_v, wg_v, wu_v, wd_v, z_v, halo_v, taps_v, px, py,
         ysrc, yq, yt, oq, ot, mix, disp, xg, part, er, ret, r1, r2, r3, r4,
         load_sem, d_send, d_recv, r_send, r_recv, ag_send, ag_recv, rs_send, rs_recv, m_send, m_recv,
         p_send, p_recv, h_sem, own_sem):
    ep = lax.axis_index("ep")
    tp = lax.axis_index("tp")
    z, c = ep // 2, ep % 2
    y, x = tp // 4, tp % 4
    xm, xp, ym, yp = (x + 3) % 4, (x + 1) % 4, (y + 3) % 4, (y + 1) % 4
    x2, y2 = (x + 2) % 4, (y + 2) % 4
    near = {"x+": (ep, y * 4 + xp), "x-": (ep, y * 4 + xm), "y+": (ep, yp * 4 + x), "y-": (ep, ym * 4 + x)}

    def ep_at(dz, dc):
        return ((z + dz) % NZ) * 2 + (c + dc) % 2

    barrier = pltpu.get_barrier_semaphore()
    for dev in near.values():
        pl.semaphore_signal(barrier, inc=1, device_id=dev, device_id_type=MESH)
    for dz in range(NZ):
        for dc in range(2):
            if dz or dc:
                pl.semaphore_signal(barrier, inc=1, device_id=(ep_at(dz, dc), tp), device_id_type=MESH)

    half = pl.ds(pl.multiple_of(c * 512, 512), 512)
    loads = {}
    for n, (name, src, dst) in enumerate([
        ("px", proj.at[half], px.at[x, half]), ("py", proj.at[half], py.at[y, half]),
        ("ci", conv_in, ci_v), ("ig", in_gate, ig_v), ("og", out_gate, og_v),
        ("wg", wg.at[0], wg_v), ("wu", wu.at[0], wu_v), ("wd", wd.at[0], wd_v),
    ]):
        loads[name] = pltpu.make_async_copy(src, dst, load_sem.at[n])
        loads[name].start()

    r_all = routes[...].astype(F32)
    r0, r1_ = r_all[0:1, :], r_all[1:2, :]
    eidx = lax.broadcasted_iota(jnp.int32, (32, 256), 0).astype(F32)
    eq0, eq1 = eidx == r0, eidx == r1_
    hit = jnp.where(eq0, 1.0, 0.0) + jnp.where(eq1, 1.0, 0.0)
    before = lax.broadcasted_iota(jnp.int32, (256, 256), 0) < lax.broadcasted_iota(jnp.int32, (256, 256), 1)
    earlier = jnp.dot(hit.astype(BF16), jnp.where(before, 1.0, 0.0).astype(BF16), preferred_element_type=F32)
    p0 = r0 * 32.0 + jnp.sum(jnp.where(eq0, earlier, 0.0), axis=0, keepdims=True)
    p1 = r1_ * 32.0 + jnp.sum(jnp.where(eq1, earlier, 0.0), axis=0, keepdims=True)
    slot = lax.broadcasted_iota(jnp.int32, (1024, 256), 0).astype(F32)
    onehot = jnp.where((slot == p0) | (slot == p1), 1.0, 0.0).astype(BF16)
    disp[...] = jnp.dot(onehot, tokens[...], preferred_element_type=F32).astype(BF16).reshape(32, 32, 128)

    loads["ci"].wait()
    loads["ig"].wait()
    z_v[...] = (ci_v[...].astype(F32) * ig_v[...].astype(F32)).astype(BF16)
    pl.semaphore_wait(barrier, 35)
    halo = pltpu.make_async_remote_copy(
        z_v.at[:, 1920:2048], halo_v, h_sem.at[0], h_sem.at[1],
        device_id=((ep + 1) % 32, tp), device_id_type=MESH)
    halo.start()

    own_in = pltpu.make_async_copy(disp.at[ep], xg.at[0, y, x, 0], own_sem.at[0])
    own_in.start()
    for off in OFFS:
        for dc in range(2):
            if off == 0 and dc == 0:
                continue
            pos = ORDER[off] * 2 + dc
            dst = ep_at((NZ - off) % NZ, dc)
            pltpu.make_async_remote_copy(
                disp.at[dst], xg.at[pos // 8, y, x, pos % 8], d_send.at[0], d_recv.at[pos // 8],
                device_id=(dst, tp), device_id_type=MESH).start()

    tap_rows = jnp.concatenate([taps[...], jnp.zeros((125, 1024), F32)], axis=0)
    taps_v[...] = tap_rows.T
    t_all = taps_v[pl.ds(pl.multiple_of(tp * 64, 64), 64), :]
    t0, t1, t2 = t_all[:, 0:1], t_all[:, 1:2], t_all[:, 2:3]
    loads["og"].wait()

    def make_y(n):
        here = z_v[:, n * 512:(n + 1) * 512].astype(F32)
        if n:
            edge = z_v[:, n * 512 - 128:n * 512].astype(F32)
        else:
            edge = jnp.where(ep > 0, halo_v[...].astype(F32), 0.0)
        longer = jnp.concatenate([edge, here], axis=1)
        conv = t0 * here + t1 * pltpu.roll(longer, 1, 1)[:, 128:] + t2 * pltpu.roll(longer, 2, 1)[:, 128:]
        gated = (og_v[:, n * 512:(n + 1) * 512].astype(F32) * conv).astype(BF16)
        for g in range(4):
            ysrc[n, g] = gated[:, g * 128:(g + 1) * 128]
        yq[n, y, x] = ysrc[n, y if n % 2 else x]

    def start(copies):
        for cp in copies:
            cp.start()

    def arrived(ref, sem):
        pltpu.make_async_remote_copy(ref, ref, h_sem.at[0], sem, device_id=near["x+"], device_id_type=MESH).wait_recv()

    def left(ref, sem):
        pltpu.make_async_remote_copy(ref, ref, sem, h_sem.at[1], device_id=near["x+"], device_id_type=MESH).wait_send()

    def gather(buf, size, job):
        h, q = size // 2, size // 4
        def send(n, ref, way):
            return pltpu.make_async_remote_copy(
                ref, ref, ag_send.at[n // 8], ag_recv.at[job, n // 4], device_id=near[way], device_id_type=MESH)
        start([
            send(0, buf.at[y, x, 0:h], "x+"), send(1, buf.at[y, x, 0:h], "x-"),
            send(2, buf.at[y, x, h:size], "y+"), send(3, buf.at[y, x, h:size], "y-")])
        yield
        arrived(buf.at[0, 0:2], ag_recv.at[job, 0])
        start([
            send(4, buf.at[y, xm, 0:q], "x+"), send(5, buf.at[y, xp, q:h], "x-"),
            send(6, buf.at[ym, x, h:h + q], "y+"), send(7, buf.at[yp, x, h + q:size], "y-")])
        yield
        arrived(buf.at[0, 0], ag_recv.at[job, 1])
        start([
            send(8, buf.at[y, :, 0:h], "y+"), send(9, buf.at[y, :, 0:h], "y-"),
            send(10, buf.at[:, x, h:size], "x+"), send(11, buf.at[:, x, h:size], "x-")])
        yield
        arrived(buf.at[0:2], ag_recv.at[job, 2])
        start([
            send(12, buf.at[ym, :, 0:q], "y+"), send(13, buf.at[yp, :, q:h], "y-"),
            send(14, buf.at[:, xm, h:h + q], "x+"), send(15, buf.at[:, xp, h + q:size], "x-")])
        yield
        arrived(buf.at[0], ag_recv.at[job, 3])

    def proj_job():
        lo = pl.ds(pl.multiple_of(c * 512, 512), 256)
        hi = pl.ds(pl.multiple_of(c * 512 + 256, 256), 256)
        partner = (z * 2 + (c + 1) % 2, tp)

        def send(n, ref, dev):
            return pltpu.make_async_remote_copy(
                ref, ref, p_send.at[n // 8], p_recv.at[n // 4], device_id=dev, device_id_type=MESH)

        loads["px"].wait()
        loads["py"].wait()
        start([
            send(0, px.at[x, half], near["x+"]), send(1, px.at[x, half], near["x-"]),
            send(2, py.at[y, half], near["y+"]), send(3, py.at[y, half], near["y-"])])
        yield
        arrived(px.at[0:2], p_recv.at[0])
        start([
            send(4, px.at[xm, lo], near["x+"]), send(5, px.at[xp, hi], near["x-"]),
            send(6, py.at[ym, lo], near["y+"]), send(7, py.at[yp, hi], near["y-"])])
        yield
        arrived(px.at[0], p_recv.at[1])
        start([send(8, px.at[:, half], partner), send(9, py.at[:, half], partner)])
        yield
        arrived(px, p_recv.at[2])
        yield

    def mixer_job(n):
        a, b = 2 * n, 2 * n + 1
        if n == 0:
            halo.wait_recv()
        make_y(a)
        make_y(b)

        def send(m, src, dst, way):
            return pltpu.make_async_remote_copy(
                src, dst, m_send.at[n], m_recv.at[n, M_GROUP[m // 4]], device_id=near[way], device_id_type=MESH)

        start([
            send(0, ysrc.at[a, x2, 0:32], yt.at[a, 0], "x+"), send(1, ysrc.at[a, x2, 32:64], yt.at[a, 1], "x-"),
            send(2, ysrc.at[b, y2, 0:32], yt.at[b, 0], "y+"), send(3, ysrc.at[b, y2, 32:64], yt.at[b, 1], "y-")])
        start([
            send(4, ysrc.at[a, xp], yq.at[a, y, x], "x+"), send(5, ysrc.at[a, xm], yq.at[a, y, x], "x-"),
            send(6, ysrc.at[b, yp], yq.at[b, y, x], "y+"), send(7, ysrc.at[b, ym], yq.at[b, y, x], "y-")])
        yield
        arrived(yq.at[a, 0, 0:2], m_recv.at[n, 0])
        start([
            send(8, yt.at[a, 0], yq.at[a, y, xm, 0:32], "x+"), send(9, yt.at[a, 1], yq.at[a, y, xp, 32:64], "x-"),
            send(10, yt.at[b, 0], yq.at[b, ym, x, 0:32], "y+"), send(11, yt.at[b, 1], yq.at[b, yp, x, 32:64], "y-")])
        yield
        arrived(yq.at[a, 0:2, 0:3], m_recv.at[n, 1])
        start([
            send(12, yq.at[a, y], yq.at[a, y], "y+"), send(13, yq.at[a, y], yq.at[a, y], "y-"),
            send(14, yq.at[b, :, x], yq.at[b, :, x], "x+"), send(15, yq.at[b, :, x], yq.at[b, :, x], "x-")])
        yield
        arrived(yq.at[a], m_recv.at[n, 2])
        start([
            send(16, yq.at[a, ym, :, 0:32], yq.at[a, ym, :, 0:32], "y+"),
            send(17, yq.at[a, yp, :, 32:64], yq.at[a, yp, :, 32:64], "y-"),
            send(18, yq.at[b, :, xm, 0:32], yq.at[b, :, xm, 0:32], "x+"),
            send(19, yq.at[b, :, xp, 32:64], yq.at[b, :, xp, 32:64], "x-")])
        yield
        arrived(yq.at[a, 0:2], m_recv.at[n, 3])
        for k, pw in ((a, px), (b, py)):
            full = jnp.concatenate([yq[k, i, j] for i in range(4) for j in range(4)], axis=0)
            rows = full.astype(F32).T.astype(BF16)
            block = jnp.dot(rows, jnp.concatenate([pw[g] for g in range(4)], axis=1),
                            preferred_element_type=F32).astype(BF16)
            for g in range(4):
                oq[k, g] = block[:, g * 128:(g + 1) * 128]
            mine = y if k % 2 else x
            mix[k, mine] = oq[k, mine]
        start([
            send(20, oq.at[a, x2, 0:64], ot.at[a, 0], "x+"), send(21, oq.at[a, x2, 64:128], ot.at[a, 1], "x-"),
            send(22, oq.at[b, y2, 0:64], ot.at[b, 0], "y+"), send(23, oq.at[b, y2, 64:128], ot.at[b, 1], "y-")])
        start([
            send(24, oq.at[a, xp], mix.at[a, x], "x+"), send(25, oq.at[a, xm], mix.at[a, x], "x-"),
            send(26, oq.at[b, yp], mix.at[b, y], "y+"), send(27, oq.at[b, ym], mix.at[b, y], "y-")])
        yield
        arrived(yq.at[a, 0], m_recv.at[n, 4])
        start([
            send(28, ot.at[a, 0], mix.at[a, xm, 0:64], "x+"), send(29, ot.at[a, 1], mix.at[a, xp, 64:128], "x-"),
            send(30, ot.at[b, 0], mix.at[b, ym, 0:64], "y+"), send(31, ot.at[b, 1], mix.at[b, yp, 64:128], "y-")])
        yield
        arrived(yq.at[a, 0:3], m_recv.at[n, 5])
        for k in (a, b):
            mixed_ref[k * 512:(k + 1) * 512, :] = mix[k].reshape(512, 128)
        yield

    def gather_job(n):
        if n == 0:
            own_in.wait()
        arrived(xg.at[n, 0, 0, 0:7 if n == 0 else 8], d_recv.at[n])
        yield from gather(xg.at[n], 8, n)
        yield

    def experts(n):
        if "wg" in loads:
            for name in ("wg", "wu", "wd"):
                loads.pop(name).wait()
        cols = [xg[n, i, j].reshape(256, 128) for i in range(4) for j in range(4)]
        squares = jnp.square(cols[0].astype(F32))
        for col in cols[1:]:
            squares = squares + jnp.square(col.astype(F32))
        scale = lax.rsqrt(jnp.sum(squares, axis=1, keepdims=True) / 2048.0 + EPSILON)
        rows = jnp.concatenate(cols, axis=1)
        gate = scale * jnp.dot(rows, wg_v[...], preferred_element_type=F32)
        up = scale * jnp.dot(rows, wu_v[...], preferred_element_type=F32)
        hidden = (gate * (1.0 / (1.0 + jnp.exp(-gate))) * up).astype(BF16)
        for i in range(4):
            block = jnp.dot(hidden, wd_v[:, i * 512:(i + 1) * 512], preferred_element_type=F32).astype(BF16)
            for j in range(4):
                part[n, i, j] = block[:, j * 128:(j + 1) * 128].reshape(8, 32, 128)

    def add(*refs):
        total = refs[0][...].astype(F32)
        for ref in refs[1:]:
            total = total + ref[...].astype(F32)
        return total.astype(BF16)

    own_out = pltpu.make_async_copy(er.at[0, 0], ret.at[ep], own_sem.at[1])

    def scatter_job(n):
        experts(n)
        buf = part.at[n]

        def send(m, src, dst, way):
            return pltpu.make_async_remote_copy(
                src, dst, rs_send.at[m // 8], rs_recv.at[n, m // 4], device_id=near[way], device_id_type=MESH)

        start([
            send(0, buf.at[y2, :, 0:2], r1.at[n, 0], "y+"), send(1, buf.at[y2, :, 2:4], r1.at[n, 1], "y-"),
            send(2, buf.at[:, x2, 4:6], r1.at[n, 2], "x+"), send(3, buf.at[:, x2, 6:8], r1.at[n, 3], "x-")])
        yield
        arrived(buf.at[0], rs_recv.at[n, 0])
        buf[yp, :, 0:2] = add(buf.at[yp, :, 0:2], r1.at[n, 0])
        buf[ym, :, 2:4] = add(buf.at[ym, :, 2:4], r1.at[n, 1])
        buf[:, xp, 4:6] = add(buf.at[:, xp, 4:6], r1.at[n, 2])
        buf[:, xm, 6:8] = add(buf.at[:, xm, 6:8], r1.at[n, 3])
        start([
            send(4, buf.at[yp, :, 0:4], r2.at[n, 0], "y+"), send(5, buf.at[ym, :, 0:4], r2.at[n, 1], "y-"),
            send(6, buf.at[:, xp, 4:8], r2.at[n, 2], "x+"), send(7, buf.at[:, xm, 4:8], r2.at[n, 3], "x-")])
        yield
        arrived(buf.at[0:2], rs_recv.at[n, 1])
        buf[y, :, 0:4] = add(buf.at[y, :, 0:4], r2.at[n, 0], r2.at[n, 1])
        buf[:, x, 4:8] = add(buf.at[:, x, 4:8], r2.at[n, 2], r2.at[n, 3])
        start([
            send(8, buf.at[y, x2, 0:2], r3.at[n, 0], "x+"), send(9, buf.at[y, x2, 2:4], r3.at[n, 1], "x-"),
            send(10, buf.at[y2, x, 4:6], r3.at[n, 2], "y+"), send(11, buf.at[y2, x, 6:8], r3.at[n, 3], "y-")])
        yield
        arrived(buf.at[0, 0], rs_recv.at[n, 2])
        buf[y, xp, 0:2] = add(buf.at[y, xp, 0:2], r3.at[n, 0])
        buf[y, xm, 2:4] = add(buf.at[y, xm, 2:4], r3.at[n, 1])
        buf[yp, x, 4:6] = add(buf.at[yp, x, 4:6], r3.at[n, 2])
        buf[ym, x, 6:8] = add(buf.at[ym, x, 6:8], r3.at[n, 3])
        start([
            send(12, buf.at[y, xp, 0:4], r4.at[n, 0], "x+"), send(13, buf.at[y, xm, 0:4], r4.at[n, 1], "x-"),
            send(14, buf.at[yp, x, 4:8], r4.at[n, 2], "y+"), send(15, buf.at[ym, x, 4:8], r4.at[n, 3], "y-")])
        yield
        arrived(buf.at[0, 0:2], rs_recv.at[n, 3])
        er[n, 0:4] = add(buf.at[y, x, 0:4], r4.at[n, 0], r4.at[n, 1])
        er[n, 4:8] = add(buf.at[y, x, 4:8], r4.at[n, 2], r4.at[n, 3])
        for pos in reversed(range(n * 8, n * 8 + 8)):
            if pos == 0:
                own_out.start()
                continue
            dst = ep_at(OFFS[pos // 2], pos % 2)
            pltpu.make_async_remote_copy(
                er.at[n, pos % 8], ret.at[ep], r_send.at[0], r_recv.at[0],
                device_id=(dst, tp), device_id_type=MESH).start()
        yield

    jobs = {"P": proj_job(), "M0": mixer_job(0), "M1": mixer_job(1)}
    for n in range(NCH):
        jobs[f"G{n}"] = gather_job(n)
        jobs[f"S{n}"] = scatter_job(n)
    for item in PLAN:
        next(jobs[item])

    row = lax.broadcasted_iota(jnp.int32, (128, 256), 0)
    w_all = weights[...]
    table = jnp.where(row == 0, p0, 0.0) + jnp.where(row == 1, p1, 0.0)
    table = jnp.where(row == 2, w_all[0:1, :], table)
    table = jnp.where(row == 3, w_all[1:2, :], table)
    cols = table.T
    slot_t = lax.broadcasted_iota(jnp.int32, (256, 1024), 1).astype(F32)
    pick0 = jnp.where(slot_t == cols[:, 0:1], 1.0, 0.0).astype(BF16)
    pick1 = jnp.where(slot_t == cols[:, 1:2], 1.0, 0.0).astype(BF16)
    own_out.wait()
    arrived(ret.at[0:31], r_recv.at[0])
    home = ret[...].reshape(1024, 128)
    out_ref[...] = (cols[:, 2:3] * jnp.dot(pick0, home, preferred_element_type=F32)
                    + cols[:, 3:4] * jnp.dot(pick1, home, preferred_element_type=F32)).astype(BF16)
    halo.wait_send()
    left(disp.at[0:31], d_send.at[0])
    left(ret.at[0:31], r_send.at[0])
    left(xg.at[0, 0:3], ag_send.at[0])
    left(xg.at[0:3], ag_send.at[1])
    left(part.at[0:3], rs_send.at[0])
    left(part.at[0, 0:3], rs_send.at[1])
    left(px.at[0:3], p_send.at[0])
    left(px, p_send.at[1])
    left(px.at[0:3], m_send.at[0])
    left(px.at[0:3], m_send.at[1])


def step(conv_input, out_gate, in_gate, conv_taps, mixer_proj, token_rows, routes, route_weights,
         expert_gate, expert_up, expert_down):
    vmem = pl.BlockSpec(memory_space=pltpu.VMEM)
    hbm = pl.BlockSpec(memory_space=pl.ANY)
    dma = pltpu.SemaphoreType.DMA
    return pl.pallas_call(
        body,
        out_shape=(jax.ShapeDtypeStruct((2048, 128), BF16), jax.ShapeDtypeStruct((256, 128), BF16)),
        in_specs=[hbm, hbm, hbm, vmem, hbm, vmem, vmem, vmem, hbm, hbm, hbm],
        out_specs=(vmem, vmem),
        scratch_shapes=[
            pltpu.VMEM((64, 2048), BF16), pltpu.VMEM((64, 2048), BF16), pltpu.VMEM((64, 2048), BF16),
            pltpu.VMEM((2048, 256), BF16), pltpu.VMEM((2048, 256), BF16), pltpu.VMEM((256, 2048), BF16),
            pltpu.VMEM((64, 2048), BF16), pltpu.VMEM((64, 128), BF16), pltpu.VMEM((1024, 128), F32),
            pltpu.VMEM((4, 1024, 128), BF16), pltpu.VMEM((4, 1024, 128), BF16),
            pltpu.VMEM((4, 4, 64, 128), BF16), pltpu.VMEM((4, 4, 4, 64, 128), BF16),
            pltpu.VMEM((4, 2, 32, 128), BF16), pltpu.VMEM((4, 4, 128, 128), BF16),
            pltpu.VMEM((4, 2, 64, 128), BF16), pltpu.VMEM((4, 4, 128, 128), BF16),
            pltpu.VMEM((32, 32, 128), BF16),
            pltpu.VMEM((NCH, 4, 4, 8, 32, 128), BF16),
            pltpu.VMEM((NCH, 4, 4, 8, 32, 128), BF16),
            pltpu.VMEM((NCH, 8, 32, 128), BF16),
            pltpu.VMEM((32, 32, 128), BF16),
            pltpu.VMEM((NCH, 4, 4, 2, 32, 128), BF16),
            pltpu.VMEM((NCH, 4, 4, 4, 32, 128), BF16),
            pltpu.VMEM((NCH, 4, 2, 32, 128), BF16),
            pltpu.VMEM((NCH, 4, 4, 32, 128), BF16),
            dma((8,)), dma((1,)), dma((NCH,)), dma((1,)), dma((1,)),
            dma((2,)), dma((NCH, 4)), dma((2,)), dma((NCH, 4)), dma((2,)), dma((2, 6)),
            dma((2,)), dma((3,)), dma((2,)), dma((2,)),
        ],
        compiler_params=pltpu.CompilerParams(
            collective_id=0, has_side_effects=True, vmem_limit_bytes=60 * 1024 * 1024),
    )(conv_input, out_gate, in_gate, conv_taps, mixer_proj, token_rows, routes.T, route_weights.T,
      expert_gate, expert_up, expert_down)


def solution(mesh):
    return jax.shard_map(
        step,
        mesh=mesh,
        in_specs=(
            P("tp", "ep"), P("tp", "ep"), P("tp", "ep"), P(), P(None, "tp"), P("ep", "tp"),
            P("ep", None), P("ep", None), P("ep", None, "tp"), P("ep", None, "tp"), P("ep", "tp", None),
        ),
        out_specs=(P("ep", "tp"), P("ep", "tp")),
        check_vma=False,
    )
```

time: 243 us -> 90.2 us (0.37)
  blocking collectives: 97.7 us -> 0 us
  Pallas kernels: 0 us -> 86.8 us
  waiting for transfers between devices: 73.6 us -> 0 us
  starting transfers between devices: 16 us -> 0 us
  matrix products: 15.4 us -> 0 us
  other arithmetic: 13.6 us -> 0 us
  between operations: 14.2 us -> 0.65 us
  local copies, waits for them, and re-layouts: 12.4 us -> 2.53 us
    all_to_all x2 -> x0, blocking collectives: 97.7 us -> none  [the longest x1 58.8 us: sent_and_summed(): lax.all_to_all(blocks, axis, split_axis=0, concat_axis=0, tiled=True)]
    pallas_call x0 -> x1, Pallas kernels: none -> 86.8 us  [step(): pl.pallas_call(body, out_shape=(jax.ShapeDtypeStruct((2048, 128), BF16),...]
    all_gather x2 -> x0, waiting for transfers between devices: 58.8 us -> none  [the longest x1 55.6 us: body(): part_in = lax.all_gather(arrived, 'tp', axis=1, tiled=True)]
    dot_general x3 -> x0, matrix products: 15.4 us -> none  [the longest x1 8.82 us: body(): lax.dot_general(down_weight, hidden, (((0,), (1,)), ((), ())), preferred_...]
    all_to_all x1 -> x0, waiting for transfers between devices: 14.6 us -> none  [body(): lax.all_to_all(expert_rows, 'ep', split_axis=1, concat_axis=1, tiled=True)]
    all_to_all x1 -> x0, starting transfers between devices: 13.7 us -> none  [body(): lax.all_to_all(expert_rows, 'ep', split_axis=1, concat_axis=1, tiled=True)]
    reduce_sum x4 -> x0, other arithmetic: 8.3 us -> none  [the longest x1 3.94 us: sent_and_summed(): return arrived.astype(jnp.float32).sum(axis=0)]
    scatter x1 -> x0, local copies, waits for them, and re-layouts: 4.9 us -> none  [body(): jnp.zeros((slot_total, cols_part), jnp.bfloat16).at[places]]
  transfers between devices with their start and end apart: 4 -> 0, of which waited for: 4 -> 0; matrix products, arithmetic and copies ran while one was open for 12% -> 0% of each run, Pallas kernels for 0% -> 0%
where the time goes in v1:
time: 90.2 us; the launch traced here: 90 us
  Pallas kernels  86.8 us (96%)
  local copies, waits for them, and re-layouts  2.53 us (3%)
    pallas_call x1, Pallas kernels, step(): pl.pallas_call(body, out_shape=(jax.ShapeDtypeStruct((2048, 128), BF16),...  86.8 us
    unnamed x4, local copies, waits for them, and re-layouts  2.53 us

profile of v1, /device:TPU:1, one launch (start us, length us, event | category | flops | bytes accessed | tf_op | source)
XLA Modules:
  0.0 90.0 jit_solution(7415082816114181637)
XLA Ops:
  0.6 86.8 %shard_map.122 = (bf16[2048,128]{1,0:T(8,128)(2,1)}, bf16[256,128]{1,0:T(8,128)(2,1)}) custom-call(bf16[64,2048]{1,0:T(8,128)(2,1)} %conv_in.1, bf16[64,2048]{1,0:T(8,128)(2,1)} %out_gate.1, bf16[64,2048]{1,0:T(8,128)(2,1)} %in_gate.1, f32[3,1024]{1,0:T(4,128)} %taps.1, bf16[1024,128]{1,0:T(8,128)(2,1)} %proj.1, bf16[256,128]{1,0:T(8,128)(2,1)} %tokens.1, ...), custom_call_target="tpu_custom_call" | custom-call | tf_op jit(solution)/shard_map/pallas_call | solution.py:361
  87.4 0.0 copy-start
  87.4 1.9 %copy.15 = bf16[2048,128]{1,0:T(8,128)(2,1)} copy(bf16[2048,128]{1,0:T(8,128)(2,1)} %get-tuple-element.4) | data formatting | bytes 1048576
  89.3 0.0 copy-done
  89.3 0.6 copy.16
Async XLA Ops:
  87.4 1.9 %copy-start = (bf16[256,128]{1,0:T(8,128)(2,1)S(1)}, bf16[256,128]{1,0:T(8,128)(2,1)}, u32[]{:S(2)}) copy-start(bf16[256,128]{1,0:T(8,128)(2,1)} %get-tuple-element.5) | copy-start | bytes 196612

commit v2 on v1

--- a/solution.py
+++ b/solution.py
@@ -16,10 +16,10 @@
 ORDER = {o: n for n, o in enumerate(OFFS)}
 
 PLAN = [
-    "M1", "P", "M1", "G0", "P", "M0", "G0", "G1", "M1", "G0", "M0", "G2", "G3", "G1", "G0", "G2",
-    "G3", "G1", "G3", "G1", "G2", "G0", "G1", "G3", "S1", "S0", "G2", "G3", "S3", "S1", "G2", "S2",
-    "S3", "S1", "S2", "S1", "S3", "S0", "P", "S2", "S3", "S1", "M0", "S0", "S2", "M1", "S3", "M0",
-    "S0", "P", "S2", "M1", "M0", "S0", "M1", "M0", "M0", "M1",
+    "D", "P", "M1", "M0", "M0", "M1", "P", "G0", "M0", "G0", "G1", "M1", "G0", "G1", "G2", "G3",
+    "M1", "G0", "G2", "G3", "G1", "G3", "G1", "G2", "G1", "G3", "S1", "G0", "G2", "S0", "G3", "P",
+    "S3", "G2", "S1", "S2", "S3", "S1", "S2", "S1", "S3", "S0", "S1", "S2", "S3", "M0", "S0", "P",
+    "S2", "M1", "S3", "S0", "S2", "M0", "S0", "M1", "M0", "M0", "M1",
 ]
 M_GROUP = [0, 1, 1, 2, 3, 4, 5, 5]
 
@@ -72,31 +72,13 @@
     onehot = jnp.where((slot == p0) | (slot == p1), 1.0, 0.0).astype(BF16)
     disp[...] = jnp.dot(onehot, tokens[...], preferred_element_type=F32).astype(BF16).reshape(32, 32, 128)
 
-    loads["ci"].wait()
-    loads["ig"].wait()
-    z_v[...] = (ci_v[...].astype(F32) * ig_v[...].astype(F32)).astype(BF16)
-    pl.semaphore_wait(barrier, 35)
-    halo = pltpu.make_async_remote_copy(
-        z_v.at[:, 1920:2048], halo_v, h_sem.at[0], h_sem.at[1],
-        device_id=((ep + 1) % 32, tp), device_id_type=MESH)
-    halo.start()
-
-    own_in = pltpu.make_async_copy(disp.at[ep], xg.at[0, y, x, 0], own_sem.at[0])
-    own_in.start()
-    for off in OFFS:
-        for dc in range(2):
-            if off == 0 and dc == 0:
-                continue
-            pos = ORDER[off] * 2 + dc
-            dst = ep_at((NZ - off) % NZ, dc)
-            pltpu.make_async_remote_copy(
-                disp.at[dst], xg.at[pos // 8, y, x, pos % 8], d_send.at[0], d_recv.at[pos // 8],
-                device_id=(dst, tp), device_id_type=MESH).start()
-
     tap_rows = jnp.concatenate([taps[...], jnp.zeros((125, 1024), F32)], axis=0)
     taps_v[...] = tap_rows.T
     t_all = taps_v[pl.ds(pl.multiple_of(tp * 64, 64), 64), :]
     t0, t1, t2 = t_all[:, 0:1], t_all[:, 1:2], t_all[:, 2:3]
+    loads["ci"].wait()
+    loads["ig"].wait()
+    z_v[...] = (ci_v[...].astype(F32) * ig_v[...].astype(F32)).astype(BF16)
     loads["og"].wait()
 
     def make_y(n):
@@ -112,6 +94,30 @@
             ysrc[n, g] = gated[:, g * 128:(g + 1) * 128]
         yq[n, y, x] = ysrc[n, y if n % 2 else x]
 
+    for n in range(1, NCH):
+        make_y(n)
+
+    pl.semaphore_wait(barrier, 35)
+
+    halo = pltpu.make_async_remote_copy(
+        z_v.at[:, 1920:2048], halo_v, h_sem.at[0], h_sem.at[1],
+        device_id=((ep + 1) % 32, tp), device_id_type=MESH)
+    own_in = pltpu.make_async_copy(disp.at[ep], xg.at[0, y, x, 0], own_sem.at[0])
+
+    def dispatch_job():
+        halo.start()
+        own_in.start()
+        for off in OFFS:
+            for dc in range(2):
+                if off == 0 and dc == 0:
+                    continue
+                pos = ORDER[off] * 2 + dc
+                dst = ep_at((NZ - off) % NZ, dc)
+                pltpu.make_async_remote_copy(
+                    disp.at[dst], xg.at[pos // 8, y, x, pos % 8], d_send.at[0], d_recv.at[pos // 8],
+                    device_id=(dst, tp), device_id_type=MESH).start()
+        yield
+
     def start(copies):
         for cp in copies:
             cp.start()
@@ -178,8 +184,7 @@
         a, b = 2 * n, 2 * n + 1
         if n == 0:
             halo.wait_recv()
-        make_y(a)
-        make_y(b)
+            make_y(0)
 
         def send(m, src, dst, way):
             return pltpu.make_async_remote_copy(
@@ -319,7 +324,7 @@
                 device_id=(dst, tp), device_id_type=MESH).start()
         yield
 
-    jobs = {"P": proj_job(), "M0": mixer_job(0), "M1": mixer_job(1)}
+    jobs = {"D": dispatch_job(), "P": proj_job(), "M0": mixer_job(0), "M1": mixer_job(1)}
     for n in range(NCH):
         jobs[f"G{n}"] = gather_job(n)
         jobs[f"S{n}"] = scatter_job(n)

time: 90.2 us -> 91.8 us (1.018)
  Pallas kernels: 86.8 us -> 88.5 us
    pallas_call x1, Pallas kernels: 86.8 us -> 88.5 us  [step(): pl.pallas_call(body, out_shape=(jax.ShapeDtypeStruct((2048, 128), BF16),...]
where the time goes in v2:
time: 91.8 us; the launch traced here: 91.6 us
  Pallas kernels  88.5 us (96%)
  local copies, waits for them, and re-layouts  2.53 us (3%)
    pallas_call x1, Pallas kernels, step(): pl.pallas_call(body, out_shape=(jax.ShapeDtypeStruct((2048, 128), BF16),...  88.5 us
    unnamed x4, local copies, waits for them, and re-layouts  2.53 us

profile of v2, /device:TPU:1, one launch (start us, length us, event | category | flops | bytes accessed | tf_op | source)
XLA Modules:
  0.0 91.6 jit_solution(5114280440521358190)
XLA Ops:
  0.6 88.5 %shard_map.122 = (bf16[2048,128]{1,0:T(8,128)(2,1)}, bf16[256,128]{1,0:T(8,128)(2,1)}) custom-call(bf16[64,2048]{1,0:T(8,128)(2,1)} %conv_in.1, bf16[64,2048]{1,0:T(8,128)(2,1)} %out_gate.1, bf16[64,2048]{1,0:T(8,128)(2,1)} %in_gate.1, f32[3,1024]{1,0:T(4,128)} %taps.1, bf16[1024,128]{1,0:T(8,128)(2,1)} %proj.1, bf16[256,128]{1,0:T(8,128)(2,1)} %tokens.1, ...), custom_call_target="tpu_custom_call" | custom-call | tf_op jit(solution)/shard_map/pallas_call | solution.py:366
  89.1 0.0 copy-start
  89.1 1.9 %copy.15 = bf16[2048,128]{1,0:T(8,128)(2,1)} copy(bf16[2048,128]{1,0:T(8,128)(2,1)} %get-tuple-element.4) | data formatting | bytes 1048576
  91.0 0.0 copy-done
  91.0 0.6 copy.16
Async XLA Ops:
  89.1 1.9 %copy-start = (bf16[256,128]{1,0:T(8,128)(2,1)S(1)}, bf16[256,128]{1,0:T(8,128)(2,1)}, u32[]{:S(2)}) copy-start(bf16[256,128]{1,0:T(8,128)(2,1)} %get-tuple-element.5) | copy-start | bytes 196612
